TPU v7x, 32 devices: a whole 2x2x4 slice. The times are simulated.
32 devices in a mesh: ep: 8 (over z, x), tp: 4 (over y, core).
Axes of the slice: x: 2, y: 2, z: 4, core: 2. Of those that a mesh axis runs over, the one named last changes fastest.
Arguments:
- mixer_input: bfloat16 [1024, 2048], P('ep'), may hold values from -6 to 6
- mixer_gain: float32 [2048], replicated, may hold values from 0.1 to 1.9
- query_weight: bfloat16 [2048, 2048], P(None, 'tp'), may hold values from -0.125 to 0.125
- key_weight: bfloat16 [2048, 2048], P(None, 'tp'), may hold values from -0.125 to 0.125
- value_weight: bfloat16 [2048, 2048], P(None, 'tp'), may hold values from -0.125 to 0.125
- score_offset: float32 [16], P('tp'), may hold values from -8.6 to -4
- out_weight: bfloat16 [2048, 2048], P(None, 'tp'), may hold values from -1.3203125 to 1.3203125
- expert_input: bfloat16 [1024, 2048], P('ep'), may hold values from -6 to 6
- expert_gain: float32 [2048], replicated, may hold values from 0.1 to 1.9
- route_ids: int32 [1024, 2], P('ep'), may hold values from 0 to 7, as said below
- route_weights: float32 [1024, 2], P('ep'), may hold values from 0.1 to 1
- gate_weight: bfloat16 [8, 2048, 2048], P('ep', None, 'tp'), may hold values from -0.125 to 0.125
- up_weight: bfloat16 [8, 2048, 2048], P('ep', None, 'tp'), may hold values from -0.125 to 0.125
- down_weight: bfloat16 [8, 2048, 2048], P('ep', 'tp'), may hold values from -0.1875 to 0.1875
Outputs:
- mixer_output: bfloat16 [1024, 2048], P('ep', 'tp')
- expert_output: bfloat16 [1024, 2048], P('ep', 'tp')
Inputs may be any that keep to these rules, and one draw needn't show every extreme that they name: `route_ids`: each row names two different experts of one group; group g holds experts g * 2 to g * 2 + 1. Among the rows of one ep index no expert is named more than 64 times, and in every draw the experts of some group are each named exactly 64 times by the rows of every ep index.
All inputs are finite; a program needn't handle non-finite values.
Results may differ from a plain program's by a relative error of at most 0.019.
Values may be sent and summed in bfloat16 or wider, within the bound.
A program may use at most 64 MiB of HBM per device.

v0:
```python
import functools

import jax
import jax.numpy as jnp
from jax import lax
from jax.experimental import pallas as pl
from jax.experimental.pallas import tpu as pltpu
from jax.sharding import PartitionSpec as P

HD = 128
SUB = 64
GROUPS = 4


epsilon = 1e-06


def rms_rows(rows_in, gain):
    values_f = rows_in.astype(jnp.float32)
    scaled = values_f * lax.rsqrt(jnp.mean(values_f * values_f, axis=-1, keepdims=True) + epsilon)
    return (scaled * gain).astype(jnp.bfloat16)


def token_mixer(
    mixer_input, mixer_gain, query_weight, key_weight, value_weight, score_offset, out_weight
):
    rows_here = mixer_input.shape[0]
    normed = rms_rows(mixer_input, mixer_gain)
    queries = jnp.dot(normed, query_weight, preferred_element_type=jnp.float32).astype(jnp.bfloat16)
    key_rows = jnp.dot(normed, key_weight, preferred_element_type=jnp.float32).astype(jnp.bfloat16)
    value_rows = jnp.dot(normed, value_weight, preferred_element_type=jnp.float32).astype(
        jnp.bfloat16
    )
    heads_here = queries.shape[1] // HD
    blocks = lax.axis_size("ep")
    my_block = lax.axis_index("ep")
    suffix_ones = jnp.tril(jnp.ones((SUB, SUB), jnp.float32))
    query_sets = (
        (queries, my_block * rows_here + jnp.arange(rows_here, dtype=jnp.int32), my_block),
    )

    def attend_set(query_flat, query_pos, key_heads, value_heads, shards):
        query_count = query_flat.shape[0]
        query_heads = query_flat.reshape(query_count, heads_here, HD)
        scores = jnp.einsum(
            "qhd,bkhd->bhqk", query_heads, key_heads, preferred_element_type=jnp.float32
        )
        scores = scores * HD ** (-0.5) + score_offset[None, :, None, None]
        key_pos = jnp.arange(shards * rows_here, dtype=jnp.int32).reshape(shards, 1, 1, rows_here)
        causal = key_pos < query_pos.reshape(1, 1, query_count, 1)
        log_keep = jnp.where(causal, jax.nn.log_sigmoid(-scores), 0.0)
        within = jnp.einsum(
            "bhqns,sr->bhqnr",
            log_keep.reshape(shards, heads_here, query_count, rows_here // SUB, SUB),
            suffix_ones,
            precision=lax.Precision.HIGHEST,
        )
        sub_total = within[..., 0]
        later_subs = lax.cumsum(sub_total, axis=3, reverse=True) - sub_total
        after_sum = (within + later_subs[..., None]).reshape(
            shards, heads_here, query_count, rows_here
        ) - log_keep
        weights = jnp.where(causal, jnp.exp(jax.nn.log_sigmoid(scores) + after_sum), 0.0).astype(
            jnp.bfloat16
        )
        block_part = jnp.einsum(
            "bhqk,bkhd->bqhd", weights, value_heads, preferred_element_type=jnp.float32
        )
        keep_part = jnp.sum(sub_total, axis=3).transpose(0, 2, 1)
        return (block_part, keep_part)

    def bind_attend(query_flat, query_pos, key_heads, value_heads, shards):

        def attend(state_in):
            return attend_set(query_flat, query_pos, key_heads, value_heads, shards)

        return attend

    def untouched(state_in):
        return state_in

    initial = tuple(
        (
            (
                jnp.zeros((blocks, entry[0].shape[0], heads_here, HD), jnp.float32),
                jnp.zeros((blocks, entry[0].shape[0], heads_here), jnp.float32),
            )
            for entry in query_sets
        )
    )
    key_part = lax.all_gather(key_rows, "ep", axis=0, tiled=True)
    value_part = lax.all_gather(value_rows, "ep", axis=0, tiled=True)
    shards = key_part.shape[0] // rows_here
    first_block = jnp.int32(0) // rows_here
    key_heads = key_part.reshape(shards, rows_here, heads_here, HD)
    value_heads = value_part.reshape(shards, rows_here, heads_here, HD)
    updated = []
    for (query_flat, query_pos, limit), state_in in zip(query_sets, initial):
        attend = bind_attend(query_flat, query_pos, key_heads, value_heads, shards)
        updated.append(lax.cond(first_block <= limit, attend, untouched, state_in))
    folded = tuple(updated)
    finished = []
    for block_out, block_keep in folded:
        later_keep = lax.cumsum(block_keep, axis=0, reverse=True) - block_keep
        summed = jnp.sum(jnp.exp(later_keep)[..., None] * block_out, axis=0)
        finished.append(summed.astype(jnp.bfloat16).reshape(block_out.shape[1], heads_here * HD))
    attended = finished[0]
    mixed_out = jnp.dot(
        lax.all_gather(attended, "tp", axis=1, tiled=True),
        out_weight,
        preferred_element_type=jnp.float32,
    )
    return mixed_out.astype(jnp.bfloat16)


def finish_expert(gate_sum, up_sum, sources, slot_count, down_weight):
    hidden = (jax.nn.silu(gate_sum) * up_sum).astype(jnp.bfloat16)
    partial_out = jnp.dot(hidden, down_weight[0], preferred_element_type=jnp.float32)
    partial_out = partial_out.reshape(sources, slot_count, partial_out.shape[1])
    summed = lax.psum_scatter(
        partial_out.astype(jnp.bfloat16), "tp", scatter_dimension=2, tiled=True
    )
    return lax.all_to_all(summed, "ep", split_axis=0, concat_axis=0, tiled=True)


def routed_experts(
    expert_input, expert_gain, route_ids, route_weights, gate_weight, up_weight, down_weight
):
    rows_here = expert_input.shape[0]
    model_width = expert_input.shape[1]
    normed = rms_rows(expert_input, expert_gain)
    experts = lax.axis_size("ep")
    capacity = rows_here // (experts // GROUPS)
    flat_ids = route_ids.reshape(-1)
    onehot = (flat_ids[:, None] == jnp.arange(experts, dtype=jnp.int32)[None, :]).astype(jnp.int32)
    slot_index = jnp.sum((jnp.cumsum(onehot, axis=0) - 1) * onehot, axis=1)
    target = flat_ids * capacity + slot_index
    assign_row = jnp.arange(flat_ids.shape[0], dtype=jnp.int32) // 2
    source_row = jnp.full((experts * capacity,), rows_here, jnp.int32).at[target].set(assign_row)
    narrow = model_width // lax.axis_size("tp")
    own_cols = lax.dynamic_slice_in_dim(normed, lax.axis_index("tp") * narrow, narrow, 1)
    padded = jnp.concatenate([own_cols, jnp.zeros((1, narrow), jnp.bfloat16)], axis=0)
    outgoing = padded[source_row].reshape(experts, capacity, narrow)
    arrived = lax.all_to_all(outgoing, "ep", split_axis=0, concat_axis=0, tiled=True)
    row_count = arrived.shape[0] * arrived.shape[1]
    fetched = lax.all_gather(arrived, "tp", axis=2, tiled=True)
    flat_rows = fetched.reshape(row_count, fetched.shape[2])
    gate_rows = gate_weight[0]
    up_rows = up_weight[0]
    gate_sum = jnp.dot(flat_rows, gate_rows, preferred_element_type=jnp.float32)
    up_sum = jnp.dot(flat_rows, up_rows, preferred_element_type=jnp.float32)
    returned = finish_expert(gate_sum, up_sum, arrived.shape[0], arrived.shape[1], down_weight)
    out_cols = returned.shape[2]
    picked = returned.reshape(experts * capacity, out_cols)[target].astype(jnp.float32)
    picked = picked.reshape(rows_here, 2, out_cols)
    combined = jnp.sum(route_weights[:, :, None] * picked, axis=1)
    return combined.astype(jnp.bfloat16)


def on_device(
    mixer_input,
    mixer_gain,
    query_weight,
    key_weight,
    value_weight,
    score_offset,
    out_weight,
    expert_input,
    expert_gain,
    route_ids,
    route_weights,
    gate_weight,
    up_weight,
    down_weight,
):
    mixer_output = token_mixer(
        mixer_input, mixer_gain, query_weight, key_weight, value_weight, score_offset, out_weight
    )
    expert_output = routed_experts(
        expert_input, expert_gain, route_ids, route_weights, gate_weight, up_weight, down_weight
    )
    return (mixer_output, expert_output)


class Wires:
    def __init__(self, send_sems, recv_sems):
        self.send_sems = send_sems
        self.recv_sems = recv_sems
        self.started = []
        self.used = 0

    def take(self, count):
        first = self.used
        self.used += count
        return first

    def make(self, src, dst, slot, peer):
        return pltpu.make_async_remote_copy(
            src_ref=src,
            dst_ref=dst,
            send_sem=self.send_sems.at[slot],
            recv_sem=self.recv_sems.at[slot],
            device_id=peer,
            device_id_type=pl.DeviceIdType.MESH,
        )

    def send(self, src, dst, slot, peer):
        copy = self.make(src, dst, slot, peer)
        copy.start()
        self.started.append(copy)

    def arrived(self, dst, slot, peer):
        self.make(dst, dst, slot, peer).wait_recv()

    def drain(self):
        for copy in self.started:
            copy.wait_send()


WIRES = 96


def fused_kernel(
    groups,
    xa_ref, ga_ref, wq_hbm, wk_hbm, wv_hbm, off_ref, wo_hbm,
    xb_ref, gb_ref, ids_ref, rw_ref, gate_hbm, up_hbm, down_hbm,
    out_ref,
    wqkv, wo, gate, up, down, load_sems,
    nb, pick, sendb, sendw, rows_all, wt_all, wt_col,
    kv_s, q_s, kv_all, q_all, acc, kept, att_s, att,
    hid, give, core_in, keep_f, s1, first_in, mid_in, s2, final, back,
    send_sems, recv_sems,
):
    f32, bf16 = jnp.float32, jnp.bfloat16
    e = lax.axis_index("ep")
    t = lax.axis_index("tp")
    z = lax.div(e, 2)
    x = lax.rem(e, 2)
    rows = xb_ref.shape[0]
    cap = rows // 2
    mix_ref, exp_ref = out_ref.at[0], out_ref.at[1]
    narrow = mix_ref.shape[1]
    pool = groups * cap
    width = xb_ref.shape[1]
    tc = t + 1 - 2 * lax.rem(t, 2)
    ty = lax.rem(t + 2, 4)
    tyc = lax.rem(tc + 2, 4)
    across = {"ep": e + 1 - 2 * x, "tp": t}
    side = {"ep": e, "tp": ty}
    twin = {"ep": e, "tp": tc}

    def peer(step, other):
        xx = 1 - x if other else x
        return {"ep": 2 * lax.rem(z + step, groups) + xx, "tp": t}

    def zfrom(step):
        return lax.rem(z + groups - step, groups)

    def zto(step):
        return lax.rem(z + step, groups)

    loads = []
    for slot, (src, dst) in enumerate((
        (wk_hbm, wqkv.at[0]), (wv_hbm, wqkv.at[1]), (wq_hbm, wqkv.at[2]),
        (gate_hbm.at[0], gate), (up_hbm.at[0], up), (down_hbm.at[0], down), (wo_hbm, wo),
    )):
        copy = pltpu.make_async_copy(src, dst, load_sems.at[slot])
        copy.start()
        loads.append(copy)

    barrier = pltpu.get_barrier_semaphore()
    greeted = [side, twin] + [
        peer(step, other) for step in range(groups) for other in (0, 1) if step or other
    ]
    for device in greeted:
        pl.semaphore_signal(barrier, inc=1, device_id=device, device_id_type=pl.DeviceIdType.MESH)

    def norm(in_ref, gain_ref):
        vals = in_ref[...].astype(f32)
        scale = lax.rsqrt(jnp.mean(vals * vals, axis=-1, keepdims=True) + epsilon)
        return (vals * scale * gain_ref[...]).astype(bf16)

    nb[...] = norm(xb_ref, gb_ref)
    lane = lax.broadcasted_iota(jnp.int32, (rows, rows), 1)
    row = lax.broadcasted_iota(jnp.int32, (rows, rows), 0)
    id_row = jnp.broadcast_to(ids_ref[0:1, :].astype(f32), (rows, rows))
    id0 = jnp.transpose(id_row).astype(jnp.int32)
    id_row = id_row.astype(jnp.int32)
    grp = lax.div(id0, jnp.full_like(id0, 2))
    odd = (id_row - 2 * lax.div(id_row, jnp.full_like(id_row, 2))) == 1
    onehot = jnp.where(lane == grp, 1.0, 0.0)
    before = jnp.where(lane < row, 1.0, 0.0)
    count = jnp.dot(before.astype(bf16), onehot.astype(bf16), preferred_element_type=f32)
    place = jnp.sum(count * onehot, axis=1, keepdims=True)
    grp_f = grp[:, 0:1].astype(f32)
    target = grp_f * cap + place
    slots = lax.broadcasted_iota(jnp.int32, (rows, pool), 1).astype(f32)
    chosen = jnp.where(slots == target, 1.0, 0.0)
    pick[...] = chosen.astype(bf16)
    turned = jnp.transpose(chosen).astype(bf16)
    my_cols = pl.ds(pl.multiple_of(t * narrow, 128), narrow)
    sendb[...] = jnp.dot(turned, nb[:, my_cols], preferred_element_type=f32).astype(bf16)
    w0 = jnp.broadcast_to(rw_ref[0:1, :], (rows, rows))
    w1 = jnp.broadcast_to(rw_ref[1:2, :], (rows, rows))
    wx0 = jnp.where(odd, w1, w0)
    wx1 = jnp.where(odd, w0, w1)
    hi0 = wx0.astype(bf16).astype(f32)
    hi1 = wx1.astype(bf16).astype(f32)
    parts = jnp.where(row == 0, hi0, jnp.where(row == 1, wx0 - hi0, jnp.where(row == 2, hi1, wx1 - hi1)))
    wide = lax.broadcasted_iota(jnp.int32, (rows, groups * 128), 1).astype(f32)
    spread = jnp.where(wide == grp_f * 128 + place, 1.0, 0.0).astype(bf16)
    sendw[...] = jnp.dot(parts[:16, :].astype(bf16), spread, preferred_element_type=f32).astype(bf16)

    pl.semaphore_wait(barrier, len(greeted))
    wires = Wires(send_sems, recv_sems)

    def blk(xx, tt, step):
        return rows_all.at[
            pl.ds(pl.multiple_of((2 * step + xx) * cap, cap), cap),
            pl.ds(pl.multiple_of(tt * narrow, 128), narrow),
        ]

    def wsend(zz):
        return sendw.at[:, pl.ds(pl.multiple_of(zz * 128, 128), 128)]

    def part(ref, zz):
        return ref.at[pl.ds(pl.multiple_of(zz * cap, cap), cap), :]

    z_rows = wires.take(groups)
    z_wts = wires.take(groups)
    for step in range(1, groups):
        wires.send(part(sendb, zto(step)), blk(x, t, step), z_rows + step, peer(step, 0))
    blk(x, t, 0)[...] = part(sendb, z)[...]

    to_first = wires.take(groups)
    to_second = wires.take(2 * groups)
    to_twin = wires.take(4 * groups)
    wt_side = wires.take(groups)

    def share_own(step):
        here = blk(x, t, step)
        src = part(sendb, z) if step == 0 else here
        first, second = (across, side) if step % 2 == 0 else (side, across)
        wires.send(src, here, to_first + step, first)
        wires.send(src, here, to_second + 2 * step, second)
        wires.send(src, here, to_twin + 4 * step, twin)

    share_own(0)
    for step in range(groups):
        if step:
            wires.send(wsend(zto(step)), wt_all.at[2 * step + x], z_wts + step, peer(step, 0))
        wires.send(wsend(zto(step)), wt_all.at[2 * step + x], wt_side + step, peer(step, 1))
    wt_all[x] = wsend(z)[...]

    na = norm(xa_ref, ga_ref)
    heads = narrow // HD
    for which in range(3):
        loads[which].wait()
        for cut in range(2):
            made = jnp.dot(
                na, wqkv[which, :, cut * (narrow // 2):(cut + 1) * (narrow // 2)], preferred_element_type=f32
            ).astype(bf16)
            for sub in range(heads // 2):
                head = cut * (heads // 2) + sub
                piece = made[:, sub * HD:(sub + 1) * HD]
                if which < 2:
                    kv_s[head, :, which * HD:(which + 1) * HD] = piece
                else:
                    q_s[head] = piece
        if which == 1:
            z_kv = wires.take(groups)
            kv_side = wires.take(groups)
            kv_all[e] = kv_s[z]
    q_in = wires.take(2 * groups)

    def half(xx):
        return pl.ds(pl.multiple_of(xx * cap, cap), cap)

    q_all[e] = q_s[z, half(x), :]

    def from_z(step):
        wires.arrived(blk(x, t, step), z_rows + step, twin)
        share_own(step)

    def from_first(step):
        got = blk(1 - x, t, step) if step % 2 == 0 else blk(x, ty, step)
        second = side if step % 2 == 0 else across
        wires.arrived(got, to_first + step, twin)
        wires.send(got, got, to_second + 2 * step + 1, second)
        wires.send(got, got, to_twin + 4 * step + 1, twin)

    def from_second(step):
        one = blk(x, ty, step) if step % 2 == 0 else blk(1 - x, t, step)
        wires.arrived(one, to_second + 2 * step, twin)
        wires.send(one, one, to_twin + 4 * step + 2, twin)
        two = blk(1 - x, ty, step)
        wires.arrived(two, to_second + 2 * step + 1, twin)
        wires.send(two, two, to_twin + 4 * step + 3, twin)

    def from_twin(step):
        mid = ((1 - x, t), (x, ty)) if step % 2 == 0 else ((x, ty), (1 - x, t))
        for k, (xx, tt) in enumerate(((x, t), mid[0], mid[1], (1 - x, ty))):
            wires.arrived(blk(xx, tt + 1 - 2 * lax.rem(tt, 2), step), to_twin + 4 * step + k, twin)

    from_first(0)
    from_z(1)
    from_first(1)
    from_z(2)
    from_second(0)
    from_z(3)
    for step in range(1, groups):
        wires.send(kv_s.at[zto(step)], kv_all.at[e], z_kv + step, peer(step, 0))
    for step in range(groups):
        for other in (0, 1):
            if step or other:
                xx = 1 - x if other else x
                wires.send(
                    q_s.at[zto(step), half(xx), :], q_all.at[e], q_in + 2 * step + other, peer(step, other)
                )
    from_first(2)
    from_second(1)
    from_first(3)

    hrows = pool
    tile = narrow // 2

    def expert_half(h):
        m_at = slice(h * hrows, (h + 1) * hrows)

        def expert_tile(i, carry):
            n_at = pl.ds(pl.multiple_of(i * tile, 128), tile)
            g = jnp.dot(rows_all[m_at, :], gate[:, n_at], preferred_element_type=f32)
            u = jnp.dot(rows_all[m_at, :], up[:, n_at], preferred_element_type=f32)
            hid[m_at, n_at] = (g / (1.0 + jnp.exp(-g)) * u).astype(bf16)
            return carry

        lax.fori_loop(0, 2, expert_tile, 0)

    def down_cols(h, tt):
        m_at = slice(h * hrows, (h + 1) * hrows)
        at = pl.ds(pl.multiple_of(tt * narrow, 128), narrow)
        return jnp.dot(hid[m_at, :], down[:, at], preferred_element_type=f32) * wt_col[m_at, 0:1]

    core_at = wires.take(4)

    def give_half(h):
        for k, tt in ((1, tyc), (0, tc)):
            give[h, k] = down_cols(h, tt).astype(bf16)
            wires.send(give.at[h, k], core_in.at[h, k], core_at + 2 * h + k, twin)
        keep_f[h, 1] = down_cols(h, ty)
        keep_f[h, 0] = down_cols(h, t)

    first_at = wires.take(2 * groups)
    mid_at = wires.take(groups)
    home = wires.take(groups)

    def by_side(step):
        return step < 3

    def s1_rows(step, k, xx):
        h, odd_step = step // 2, step % 2
        return s1.at[h, k, pl.ds(pl.multiple_of((2 * odd_step + xx) * cap, cap), cap), :]

    def sum_core(h):
        steps = (2 * h, 2 * h + 1)
        wires.arrived(core_in.at[h, 1], core_at + 2 * h + 1, twin)
        s1[h, 1] = (keep_f[h, 1] + core_in[h, 1].astype(f32)).astype(bf16)
        for step in steps:
            way = side if by_side(step) else across
            wires.send(s1_rows(step, 1, 1 - x), first_in.at[step, 0], first_at + 2 * step, way)
        for step in steps:
            if by_side(step):
                wires.send(s1_rows(step, 1, x), first_in.at[step, 1], first_at + 2 * step + 1, side)
        wires.arrived(core_in.at[h, 0], core_at + 2 * h, twin)
        s1[h, 0] = (keep_f[h, 0] + core_in[h, 0].astype(f32)).astype(bf16)
        for step in steps:
            if not by_side(step):
                wires.send(s1_rows(step, 0, 1 - x), first_in.at[step, 1], first_at + 2 * step + 1, across)

    def sum_first(step):
        wires.arrived(first_in.at[step, 0], first_at + 2 * step, twin)
        mine = s1_rows(step, 0, 1 - x) if by_side(step) else s1_rows(step, 1, x)
        s2[step] = (mine[...].astype(f32) + first_in[step, 0].astype(f32)).astype(bf16)
        wires.send(s2.at[step], mid_in.at[step], mid_at + step, across if by_side(step) else side)

    def sum_last(step):
        wires.arrived(first_in.at[step, 1], first_at + 2 * step + 1, twin)
        wires.arrived(mid_in.at[step], mid_at + step, twin)
        final[step] = (
            s1_rows(step, 0, x)[...].astype(f32) + first_in[step, 1].astype(f32) + mid_in[step].astype(f32)
        ).astype(bf16)
        if step == 0:
            part(back, z)[...] = final[0]
        else:
            wires.send(final.at[step], part(back, z), home + step, {"ep": 2 * zfrom(step) + x, "tp": t})

    loads[3].wait()
    loads[4].wait()
    from_twin(0)
    from_twin(1)
    expert_half(0)
    for step in range(groups):
        if step:
            wires.arrived(wt_all.at[2 * step + x], z_wts + step, twin)
        wires.arrived(wt_all.at[2 * step + 1 - x], wt_side + step, twin)
    for i in range(2 * groups):
        tiles = wt_all[i].astype(f32)
        both = jnp.where(x == 0, tiles[0:1, :] + tiles[1:2, :], tiles[2:3, :] + tiles[3:4, :])
        wt_col[i * cap:(i + 1) * cap, :] = jnp.transpose(jnp.broadcast_to(both, (128, 128)))[:cap, :]
    loads[5].wait()
    give_half(0)
    from_second(2)
    from_second(3)
    wires.send(kv_s.at[z], kv_all.at[e], kv_side, across)
    for step in range(1, groups):
        kv_at = kv_all.at[2 * zfrom(step) + x]
        wires.arrived(kv_at, z_kv + step, twin)
        wires.send(kv_at, kv_at, kv_side + step, across)
    sum_core(0)
    from_twin(2)
    from_twin(3)
    expert_half(1)
    give_half(1)
    sum_core(1)
    sum_first(0)
    sum_first(1)

    for step in range(groups):
        wires.arrived(kv_all.at[2 * zfrom(step) + 1 - x], kv_side + step, twin)
        for other in (0, 1):
            if step or other:
                xx = 1 - x if other else x
                wires.arrived(q_all.at[2 * zfrom(step) + xx], q_in + 2 * step + other, twin)
    blocks = 2 * groups
    acc[...] = jnp.zeros_like(acc)
    kept[...] = jnp.zeros_like(kept)
    offset = off_ref[z]
    later = jnp.where(row > lane, 1.0, 0.0).astype(bf16)
    for kb in reversed(range(blocks)):
        low = kb * cap
        size = blocks * cap - low
        if kb == 1:
            sum_first(2)
            sum_first(3)
        queries = q_all[kb:, :, :].reshape(size, HD)
        scores = lax.dot_general(
            queries, kv_all[kb, :, :HD], (((1,), (1,)), ((), ())), preferred_element_type=f32
        )
        scores = scores * HD ** (-0.5) + offset
        r_at = lax.broadcasted_iota(jnp.int32, (size, rows), 0)
        s_at = lax.broadcasted_iota(jnp.int32, (size, rows), 1)
        causal = (r_at >= cap) | (s_at < r_at + x * cap)
        keep = -(jnp.maximum(scores, 0.0) + jnp.log1p(jnp.exp(-jnp.abs(scores))))
        masked = jnp.where(causal, keep, 0.0)
        hi = masked.astype(bf16)
        lo = (masked - hi.astype(f32)).astype(bf16)
        within = jnp.dot(hi, later, preferred_element_type=f32) + jnp.dot(
            lo, later, preferred_element_type=f32
        )
        wts = jnp.where(causal, jnp.exp(scores + keep + within), 0.0).astype(bf16)
        out = jnp.dot(wts, kv_all[kb, :, HD:], preferred_element_type=f32)
        sofar = kept[low:, :]
        acc[low:, :] = acc[low:, :] + jnp.exp(sofar) * out
        kept[low:, :] = sofar + (within[:, 0:1] + masked[:, 0:1])
    att_s[...] = acc[...].astype(bf16)

    def att_at(hh, xx):
        return att.at[half(xx), pl.ds(pl.multiple_of(t * narrow + hh * HD, HD), HD)]

    att_in = wires.take(2 * groups)
    for step in range(groups):
        for other in (0, 1):
            if step or other:
                xx = 1 - x if other else x
                wires.send(
                    part(att_s, 2 * zto(step) + xx), att_at(z, x), att_in + 2 * step + other, peer(step, other)
                )
    att_at(z, x)[...] = part(att_s, e)[...]

    sum_last(1)
    sum_last(0)

    for step in range(groups):
        for other in (0, 1):
            if step or other:
                xx = 1 - x if other else x
                wires.arrived(att_at(zfrom(step), xx), att_in + 2 * step + other, twin)

    def att_cols(tt):
        return att.at[:, pl.ds(pl.multiple_of(tt * narrow, 128), narrow)]

    att_go = wires.take(3)
    wires.send(att_cols(t), att_cols(t), att_go, side)
    wires.send(att_cols(t), att_cols(t), att_go + 1, twin)

    sum_last(2)
    sum_last(3)
    wires.arrived(att_cols(ty), att_go, twin)
    wires.send(att_cols(ty), att_cols(ty), att_go + 2, twin)
    loads[6].wait()
    wires.arrived(att_cols(tc), att_go + 1, twin)
    wires.arrived(att_cols(tyc), att_go + 2, twin)
    for cut in range(2):
        at = slice(cut * tile, (cut + 1) * tile)
        mix_ref[:, at] = jnp.dot(att[...], wo[:, at], preferred_element_type=f32).astype(bf16)

    for step in range(1, groups):
        wires.arrived(part(back, zto(step)), home + step, twin)
    exp_ref[...] = jnp.dot(pick[...], back[...], preferred_element_type=f32).astype(bf16)
    wires.drain()


def fused_on_device(
    mixer_input, mixer_gain, query_weight, key_weight, value_weight, score_offset, out_weight,
    expert_input, expert_gain, route_ids, route_weights, gate_weight, up_weight, down_weight,
):
    f32, bf16 = jnp.float32, jnp.bfloat16
    rows, width = expert_input.shape
    narrow = out_weight.shape[1]
    groups = GROUPS
    cap = rows // 2
    pool = groups * cap
    heads = narrow // HD
    ff = gate_weight.shape[2]
    vmem = pl.BlockSpec(memory_space=pltpu.VMEM)
    smem = pl.BlockSpec(memory_space=pltpu.SMEM)
    hbm = pl.BlockSpec(memory_space=pl.ANY)
    scratch = [
        pltpu.VMEM((3, width, narrow), bf16),
        pltpu.VMEM((width, narrow), bf16),
        pltpu.VMEM((width, ff), bf16),
        pltpu.VMEM((width, ff), bf16),
        pltpu.VMEM((ff, width), bf16),
        pltpu.SemaphoreType.DMA((7,)),
        pltpu.VMEM((rows, width), bf16),
        pltpu.VMEM((rows, pool), bf16),
        pltpu.VMEM((pool, narrow), bf16),
        pltpu.VMEM((16, groups * 128), bf16),
        pltpu.VMEM((2 * pool, width), bf16),
        pltpu.VMEM((2 * groups, 16, 128), bf16),
        pltpu.VMEM((2 * pool, 128), f32),
        pltpu.VMEM((heads, rows, 2 * HD), bf16),
        pltpu.VMEM((heads, rows, HD), bf16),
        pltpu.VMEM((2 * groups, rows, 2 * HD), bf16),
        pltpu.VMEM((2 * groups, cap, HD), bf16),
        pltpu.VMEM((2 * pool, HD), f32),
        pltpu.VMEM((2 * pool, HD), f32),
        pltpu.VMEM((2 * pool, HD), bf16),
        pltpu.VMEM((rows, width), bf16),
        pltpu.VMEM((2 * pool, ff), bf16),
        pltpu.VMEM((2, 2, pool, narrow), bf16),
        pltpu.VMEM((2, 2, pool, narrow), bf16),
        pltpu.VMEM((2, 2, pool, narrow), f32),
        pltpu.VMEM((2, 2, pool, narrow), bf16),
        pltpu.VMEM((groups, 2, cap, narrow), bf16),
        pltpu.VMEM((groups, cap, narrow), bf16),
        pltpu.VMEM((groups, cap, narrow), bf16),
        pltpu.VMEM((groups, cap, narrow), bf16),
        pltpu.VMEM((pool, narrow), bf16),
        pltpu.SemaphoreType.DMA((WIRES,)),
        pltpu.SemaphoreType.DMA((WIRES,)),
    ]
    both = pl.pallas_call(
        functools.partial(fused_kernel, groups),
        out_shape=jax.ShapeDtypeStruct((2, rows, narrow), bf16),
        in_specs=[vmem, vmem, hbm, hbm, hbm, smem, hbm, vmem, vmem, vmem, vmem, hbm, hbm, hbm],
        out_specs=vmem,
        scratch_shapes=scratch,
        compiler_params=pltpu.CompilerParams(
            collective_id=0, has_side_effects=True, vmem_limit_bytes=56 * 1024 * 1024
        ),
        name="fused",
    )(
        mixer_input, mixer_gain.reshape(1, width), query_weight, key_weight, value_weight, score_offset,
        out_weight, expert_input, expert_gain.reshape(1, width), route_ids.T, route_weights.T,
        gate_weight, up_weight, down_weight,
    )
    return both[0], both[1]


def fits(mesh):
    ep, tp = mesh.shape["ep"], mesh.shape["tp"]
    return ep == 2 * GROUPS and tp == 4


def solution(mesh):
    in_specs = (
        P("ep", None),
        P(),
        P(None, "tp"),
        P(None, "tp"),
        P(None, "tp"),
        P("tp"),
        P(None, "tp"),
        P("ep", None),
        P(),
        P("ep", None),
        P("ep", None),
        P("ep", None, "tp"),
        P("ep", None, "tp"),
        P("ep", "tp", None),
    )
    out_specs = (P("ep", "tp"), P("ep", "tp"))
    return jax.shard_map(
        fused_on_device if fits(mesh) else on_device, mesh=mesh, in_specs=in_specs, out_specs=out_specs, check_vma=False
    )
```

profile of v0, /device:TPU:0, one launch (start us, length us, event | category | flops | bytes accessed | tf_op | source)
XLA Modules:
  0.0 52.2 jit_solution(14324754012733336761)
XLA Ops:
  0.6 49.9 %fused.1 = bf16[2,128,512]{2,1,0:T(8,128)(2,1)} custom-call(bf16[128,2048]{1,0:T(8,128)(2,1)} %xa_ref.1, f32[1,2048]{1,0:T(1,128)} %bitcast.8, bf16[2048,512]{1,0:T(8,128)(2,1)} %wq_hbm.1, bf16[2048,512]{1,0:T(8,128)(2,1)} %wk_hbm.1, bf16[2048,512]{1,0:T(8,128)(2,1)} %wv_hbm.1, f32[4]{0:T(128)} %off_ref.1, bf16[2048,512]{1,0:T(8,128)(2,1)} %wo_hbm.1, ...), custom_call_target="tpu_custom_call" | custom-call | tf_op jit(solution)/shard_map/fused/pallas_call | solution.py:663
  50.5 1.7 %slice_bitcast_fusion = (bf16[128,512]{1,0:T(8,128)(2,1)}, bf16[128,512]{1,0:T(8,128)(2,1)}) fusion(bf16[2,128,512]{2,1,0:T(8,128)(2,1)} %fused.1), kind=kLoop, calls=%fused_computation | loop fusion | bytes 524288 | tf_op jit(solution)/shard_map/squeeze | solution.py:678
where the time goes:
time: 52.4 us; the launch traced here: 52.2 us
  Pallas kernels  49.9 us (95%)
  local copies, waits for them, and re-layouts  1.68 us (3%)
  between operations  0.64 us (1%)
    pallas_call x1, Pallas kernels, fused_on_device(): pl.pallas_call(functools.partial(fused_kernel, groups), out_shape=jax.Sha...  49.9 us
    squeeze x1, local copies, waits for them, and re-layouts, fused_on_device(): return (both[0], both[1])  1.68 us

commit v1 on v0

--- a/solution.py
+++ b/solution.py
@@ -1,4 +1,5 @@
 import functools
+import math
 
 import jax
 import jax.numpy as jnp
@@ -183,10 +184,10 @@
 
 
 class Wires:
-    def __init__(self, send_sems, recv_sems):
-        self.send_sems = send_sems
+    def __init__(self, send_sem, recv_sems):
+        self.send_sem = send_sem
         self.recv_sems = recv_sems
-        self.started = []
+        self.sent_bytes = 0
         self.used = 0
 
     def take(self, count):
@@ -194,54 +195,53 @@
         self.used += count
         return first
 
-    def make(self, src, dst, slot, peer):
-        return pltpu.make_async_remote_copy(
+    def send(self, src, dst, slot, peer, lane=0):
+        if lane == 0:
+            self.sent_bytes += math.prod(src.shape) * 2
+        pltpu.make_async_remote_copy(
             src_ref=src,
             dst_ref=dst,
-            send_sem=self.send_sems.at[slot],
+            send_sem=self.send_sem.at[lane],
             recv_sem=self.recv_sems.at[slot],
             device_id=peer,
             device_id_type=pl.DeviceIdType.MESH,
-        )
-
-    def send(self, src, dst, slot, peer):
-        copy = self.make(src, dst, slot, peer)
-        copy.start()
-        self.started.append(copy)
-
-    def arrived(self, dst, slot, peer):
-        self.make(dst, dst, slot, peer).wait_recv()
-
-    def drain(self):
-        for copy in self.started:
-            copy.wait_send()
-
-
-WIRES = 96
+        ).start()
+
+    def arrived(self, like, slot):
+        pltpu.make_async_copy(like, like, self.recv_sems.at[slot]).wait()
+
+    def drain(self, like):
+        row_bytes = like.shape[1] * 2
+        whole = like.at[pl.ds(0, self.sent_bytes // row_bytes), :]
+        pltpu.make_async_copy(whole, whole, self.send_sem.at[0]).wait()
+
+
+WIRES = 56
+LOADS = 14
 
 
 def fused_kernel(
     groups,
-    xa_ref, ga_ref, wq_hbm, wk_hbm, wv_hbm, off_ref, wo_hbm,
-    xb_ref, gb_ref, ids_ref, rw_ref, gate_hbm, up_hbm, down_hbm,
+    xa_hbm, ga_hbm, wq_hbm, wk_hbm, wv_hbm, off_hbm, wo_hbm,
+    xb_hbm, gb_hbm, ids_hbm, rw_hbm, gate_hbm, up_hbm, down_hbm,
     out_ref,
-    wqkv, wo, gate, up, down, load_sems,
+    xa_ref, ga_ref, off_ref, xb_ref, gb_ref, ids_ref, rw_ref,
+    weights, down, load_sems,
     nb, pick, sendb, sendw, rows_all, wt_all, wt_col,
-    kv_s, q_s, kv_all, q_all, acc, kept, att_s, att,
+    kv_s, q_s, kv_all, q_all, acc, att_s, att,
     hid, give, core_in, keep_f, s1, first_in, mid_in, s2, final, back,
-    send_sems, recv_sems,
+    send_sem, recv_sems,
 ):
     f32, bf16 = jnp.float32, jnp.bfloat16
     e = lax.axis_index("ep")
     t = lax.axis_index("tp")
     z = lax.div(e, 2)
     x = lax.rem(e, 2)
-    rows = xb_ref.shape[0]
+    rows, width = xb_ref.shape
     cap = rows // 2
     mix_ref, exp_ref = out_ref.at[0], out_ref.at[1]
     narrow = mix_ref.shape[1]
     pool = groups * cap
-    width = xb_ref.shape[1]
     tc = t + 1 - 2 * lax.rem(t, 2)
     ty = lax.rem(t + 2, 4)
     tyc = lax.rem(tc + 2, 4)
@@ -259,15 +259,6 @@
     def zto(step):
         return lax.rem(z + step, groups)
 
-    loads = []
-    for slot, (src, dst) in enumerate((
-        (wk_hbm, wqkv.at[0]), (wv_hbm, wqkv.at[1]), (wq_hbm, wqkv.at[2]),
-        (gate_hbm.at[0], gate), (up_hbm.at[0], up), (down_hbm.at[0], down), (wo_hbm, wo),
-    )):
-        copy = pltpu.make_async_copy(src, dst, load_sems.at[slot])
-        copy.start()
-        loads.append(copy)
-
     barrier = pltpu.get_barrier_semaphore()
     greeted = [side, twin] + [
         peer(step, other) for step in range(groups) for other in (0, 1) if step or other
@@ -275,12 +266,26 @@
     for device in greeted:
         pl.semaphore_signal(barrier, inc=1, device_id=device, device_id_type=pl.DeviceIdType.MESH)
 
+    def weight(k):
+        return weights.at[pl.ds(k * width, width), :]
+
+    wk, wv, wq, gate, up, wo = (weight(k) for k in range(6))
+    loads = {}
+    for slot, (name, from_hbm, to) in enumerate((
+        ("xb", xb_hbm, xb_ref), ("ids", ids_hbm, ids_ref), ("gb", gb_hbm, gb_ref), ("rw", rw_hbm, rw_ref),
+        ("xa", xa_hbm, xa_ref), ("ga", ga_hbm, ga_ref), ("wk", wk_hbm, wk), ("wv", wv_hbm, wv),
+        ("wq", wq_hbm, wq), ("gate", gate_hbm.at[0], gate), ("up", up_hbm.at[0], up),
+        ("down", down_hbm.at[0], down), ("wo", wo_hbm, wo), ("off", off_hbm, off_ref),
+    )):
+        loads[name] = pltpu.make_async_copy(from_hbm, to, load_sems.at[slot])
+        loads[name].start()
+
     def norm(in_ref, gain_ref):
         vals = in_ref[...].astype(f32)
         scale = lax.rsqrt(jnp.mean(vals * vals, axis=-1, keepdims=True) + epsilon)
         return (vals * scale * gain_ref[...]).astype(bf16)
 
-    nb[...] = norm(xb_ref, gb_ref)
+    loads["ids"].wait()
     lane = lax.broadcasted_iota(jnp.int32, (rows, rows), 1)
     row = lax.broadcasted_iota(jnp.int32, (rows, rows), 0)
     id_row = jnp.broadcast_to(ids_ref[0:1, :].astype(f32), (rows, rows))
@@ -298,8 +303,87 @@
     chosen = jnp.where(slots == target, 1.0, 0.0)
     pick[...] = chosen.astype(bf16)
     turned = jnp.transpose(chosen).astype(bf16)
+    loads["xb"].wait()
+    loads["gb"].wait()
+    nb[...] = norm(xb_ref, gb_ref)
     my_cols = pl.ds(pl.multiple_of(t * narrow, 128), narrow)
     sendb[...] = jnp.dot(turned, nb[:, my_cols], preferred_element_type=f32).astype(bf16)
+
+    pl.semaphore_wait(barrier, len(greeted))
+    wires = Wires(send_sem, recv_sems)
+
+    def blk(xx, tt, step):
+        return rows_all.at[
+            pl.ds(pl.multiple_of((2 * step + xx) * cap, cap), cap),
+            pl.ds(pl.multiple_of(tt * narrow, 128), narrow),
+        ]
+
+    def wsend(zz):
+        return sendw.at[:, pl.ds(pl.multiple_of(zz * 128, 128), 128)]
+
+    def part(ref, zz):
+        return ref.at[pl.ds(pl.multiple_of(zz * cap, cap), cap), :]
+
+    z_rows = wires.take(groups)
+    to_first = wires.take(groups)
+    to_second = wires.take(2 * groups)
+    to_twin = wires.take(groups)
+
+    def share_own(step):
+        here = blk(x, t, step)
+        src = part(sendb, z) if step == 0 else here
+        wires.send(src, here, to_first + step, across)
+        wires.send(src, here, to_second + 2 * step, side)
+        wires.send(src, here, to_twin + step, twin)
+
+    for step in range(1, groups):
+        wires.send(part(sendb, zto(step)), blk(x, t, step), z_rows + step, peer(step, 0))
+    share_own(0)
+    blk(x, t, 0)[...] = part(sendb, z)[...]
+
+    loads["xa"].wait()
+    loads["ga"].wait()
+    na = norm(xa_ref, ga_ref)
+    heads = narrow // HD
+    z_kv = wires.take(groups)
+    kv_side = wires.take(1)
+    q_in = wires.take(1)
+
+    def half(xx):
+        return pl.ds(pl.multiple_of(xx * cap, cap), cap)
+
+    def project(name, ref, put):
+        loads[name].wait()
+        for cut in range(2):
+            at = slice(cut * (narrow // 2), (cut + 1) * (narrow // 2))
+            made = jnp.dot(na, ref[:, at], preferred_element_type=f32).astype(bf16)
+            for sub in range(heads // 2):
+                put(cut * (heads // 2) + sub, made[:, sub * HD:(sub + 1) * HD])
+
+    def put_k(head, piece):
+        kv_s[head, :, :HD] = piece
+
+    def put_v(head, piece):
+        kv_s[head, :, HD:] = piece
+
+    def put_q(head, piece):
+        q_s[head] = piece
+
+    project("wk", wk, put_k)
+    project("wv", wv, put_v)
+    wires.send(kv_s.at[z], kv_all.at[e], kv_side, across)
+    for step in range(1, groups):
+        wires.send(kv_s.at[zto(step)], kv_all.at[e], z_kv + step, peer(step, 0))
+    kv_all[e] = kv_s[z]
+    project("wq", wq, put_q)
+    for step in range(groups):
+        for other in (0, 1):
+            if step or other:
+                xx = 1 - x if other else x
+                wires.send(q_s.at[zto(step), half(xx), :], q_all.at[e], q_in, peer(step, other))
+    q_all[e] = q_s[z, half(x), :]
+
+    loads["rw"].wait()
     w0 = jnp.broadcast_to(rw_ref[0:1, :], (rows, rows))
     w1 = jnp.broadcast_to(rw_ref[1:2, :], (rows, rows))
     wx0 = jnp.where(odd, w1, w0)
@@ -310,131 +394,50 @@
     wide = lax.broadcasted_iota(jnp.int32, (rows, groups * 128), 1).astype(f32)
     spread = jnp.where(wide == grp_f * 128 + place, 1.0, 0.0).astype(bf16)
     sendw[...] = jnp.dot(parts[:16, :].astype(bf16), spread, preferred_element_type=f32).astype(bf16)
-
-    pl.semaphore_wait(barrier, len(greeted))
-    wires = Wires(send_sems, recv_sems)
-
-    def blk(xx, tt, step):
-        return rows_all.at[
-            pl.ds(pl.multiple_of((2 * step + xx) * cap, cap), cap),
-            pl.ds(pl.multiple_of(tt * narrow, 128), narrow),
-        ]
-
-    def wsend(zz):
-        return sendw.at[:, pl.ds(pl.multiple_of(zz * 128, 128), 128)]
-
-    def part(ref, zz):
-        return ref.at[pl.ds(pl.multiple_of(zz * cap, cap), cap), :]
-
-    z_rows = wires.take(groups)
-    z_wts = wires.take(groups)
-    for step in range(1, groups):
-        wires.send(part(sendb, zto(step)), blk(x, t, step), z_rows + step, peer(step, 0))
-    blk(x, t, 0)[...] = part(sendb, z)[...]
-
-    to_first = wires.take(groups)
-    to_second = wires.take(2 * groups)
-    to_twin = wires.take(4 * groups)
-    wt_side = wires.take(groups)
-
-    def share_own(step):
-        here = blk(x, t, step)
-        src = part(sendb, z) if step == 0 else here
-        first, second = (across, side) if step % 2 == 0 else (side, across)
-        wires.send(src, here, to_first + step, first)
-        wires.send(src, here, to_second + 2 * step, second)
-        wires.send(src, here, to_twin + 4 * step, twin)
-
-    share_own(0)
-    for step in range(groups):
-        if step:
-            wires.send(wsend(zto(step)), wt_all.at[2 * step + x], z_wts + step, peer(step, 0))
-        wires.send(wsend(zto(step)), wt_all.at[2 * step + x], wt_side + step, peer(step, 1))
-    wt_all[x] = wsend(z)[...]
-
-    na = norm(xa_ref, ga_ref)
-    heads = narrow // HD
-    for which in range(3):
-        loads[which].wait()
-        for cut in range(2):
-            made = jnp.dot(
-                na, wqkv[which, :, cut * (narrow // 2):(cut + 1) * (narrow // 2)], preferred_element_type=f32
-            ).astype(bf16)
-            for sub in range(heads // 2):
-                head = cut * (heads // 2) + sub
-                piece = made[:, sub * HD:(sub + 1) * HD]
-                if which < 2:
-                    kv_s[head, :, which * HD:(which + 1) * HD] = piece
-                else:
-                    q_s[head] = piece
-        if which == 1:
-            z_kv = wires.take(groups)
-            kv_side = wires.take(groups)
-            kv_all[e] = kv_s[z]
-    q_in = wires.take(2 * groups)
-
-    def half(xx):
-        return pl.ds(pl.multiple_of(xx * cap, cap), cap)
-
-    q_all[e] = q_s[z, half(x), :]
-
-    def from_z(step):
-        wires.arrived(blk(x, t, step), z_rows + step, twin)
-        share_own(step)
-
-    def from_first(step):
-        got = blk(1 - x, t, step) if step % 2 == 0 else blk(x, ty, step)
-        second = side if step % 2 == 0 else across
-        wires.arrived(got, to_first + step, twin)
-        wires.send(got, got, to_second + 2 * step + 1, second)
-        wires.send(got, got, to_twin + 4 * step + 1, twin)
-
-    def from_second(step):
-        one = blk(x, ty, step) if step % 2 == 0 else blk(1 - x, t, step)
-        wires.arrived(one, to_second + 2 * step, twin)
-        wires.send(one, one, to_twin + 4 * step + 2, twin)
-        two = blk(1 - x, ty, step)
-        wires.arrived(two, to_second + 2 * step + 1, twin)
-        wires.send(two, two, to_twin + 4 * step + 3, twin)
-
-    def from_twin(step):
-        mid = ((1 - x, t), (x, ty)) if step % 2 == 0 else ((x, ty), (1 - x, t))
-        for k, (xx, tt) in enumerate(((x, t), mid[0], mid[1], (1 - x, ty))):
-            wires.arrived(blk(xx, tt + 1 - 2 * lax.rem(tt, 2), step), to_twin + 4 * step + k, twin)
-
-    from_first(0)
-    from_z(1)
-    from_first(1)
-    from_z(2)
-    from_second(0)
-    from_z(3)
-    for step in range(1, groups):
-        wires.send(kv_s.at[zto(step)], kv_all.at[e], z_kv + step, peer(step, 0))
+    wt_in = wires.take(1)
     for step in range(groups):
         for other in (0, 1):
             if step or other:
-                xx = 1 - x if other else x
-                wires.send(
-                    q_s.at[zto(step), half(xx), :], q_all.at[e], q_in + 2 * step + other, peer(step, other)
-                )
-    from_first(2)
-    from_second(1)
-    from_first(3)
+                wires.send(wsend(zto(step)), wt_all.at[2 * step + x], wt_in, peer(step, other), 1)
+    wt_all[x] = wsend(z)[...]
+
+    def from_z(step):
+        wires.arrived(blk(x, t, step), z_rows + step)
+        share_own(step)
+
+    def from_first(step):
+        got = blk(1 - x, t, step)
+        wires.arrived(got, to_first + step)
+        wires.send(got, got, to_second + 2 * step + 1, side)
+        wires.send(got, got, to_twin + step, twin)
+
+    def from_second(step):
+        one = blk(x, ty, step)
+        wires.arrived(one, to_second + 2 * step)
+        wires.send(one, one, to_twin + step, twin)
+
+    def from_third(step):
+        two = blk(1 - x, ty, step)
+        wires.arrived(two, to_second + 2 * step + 1)
+        wires.send(two, two, to_twin + step, twin)
+
+    def from_twin(step):
+        wires.arrived(rows_all.at[pl.ds(0, cap), :], to_twin + step)
+
+    def pass_kv(step):
+        kv_at = kv_all.at[2 * zfrom(step) + x]
+        wires.arrived(kv_at, z_kv + step)
+        wires.send(kv_at, kv_at, kv_side, across)
 
     hrows = pool
     tile = narrow // 2
 
-    def expert_half(h):
+    def expert_tile(h, i):
         m_at = slice(h * hrows, (h + 1) * hrows)
-
-        def expert_tile(i, carry):
-            n_at = pl.ds(pl.multiple_of(i * tile, 128), tile)
-            g = jnp.dot(rows_all[m_at, :], gate[:, n_at], preferred_element_type=f32)
-            u = jnp.dot(rows_all[m_at, :], up[:, n_at], preferred_element_type=f32)
-            hid[m_at, n_at] = (g / (1.0 + jnp.exp(-g)) * u).astype(bf16)
-            return carry
-
-        lax.fori_loop(0, 2, expert_tile, 0)
+        n_at = slice(i * tile, (i + 1) * tile)
+        g = jnp.dot(rows_all[m_at, :], gate[:, n_at], preferred_element_type=f32)
+        u = jnp.dot(rows_all[m_at, :], up[:, n_at], preferred_element_type=f32)
+        hid[m_at, n_at] = (g / (1.0 + jnp.exp(-g)) * u).astype(bf16)
 
     def down_cols(h, tt):
         m_at = slice(h * hrows, (h + 1) * hrows)
@@ -452,10 +455,10 @@
 
     first_at = wires.take(2 * groups)
     mid_at = wires.take(groups)
-    home = wires.take(groups)
+    home = wires.take(1)
 
     def by_side(step):
-        return step < 3
+        return step % 2 == 0
 
     def s1_rows(step, k, xx):
         h, odd_step = step // 2, step % 2
@@ -463,7 +466,7 @@
 
     def sum_core(h):
         steps = (2 * h, 2 * h + 1)
-        wires.arrived(core_in.at[h, 1], core_at + 2 * h + 1, twin)
+        wires.arrived(core_in.at[h, 1], core_at + 2 * h + 1)
         s1[h, 1] = (keep_f[h, 1] + core_in[h, 1].astype(f32)).astype(bf16)
         for step in steps:
             way = side if by_side(step) else across
@@ -471,82 +474,58 @@
         for step in steps:
             if by_side(step):
                 wires.send(s1_rows(step, 1, x), first_in.at[step, 1], first_at + 2 * step + 1, side)
-        wires.arrived(core_in.at[h, 0], core_at + 2 * h, twin)
+        wires.arrived(core_in.at[h, 0], core_at + 2 * h)
         s1[h, 0] = (keep_f[h, 0] + core_in[h, 0].astype(f32)).astype(bf16)
         for step in steps:
             if not by_side(step):
                 wires.send(s1_rows(step, 0, 1 - x), first_in.at[step, 1], first_at + 2 * step + 1, across)
 
     def sum_first(step):
-        wires.arrived(first_in.at[step, 0], first_at + 2 * step, twin)
+        wires.arrived(first_in.at[step, 0], first_at + 2 * step)
         mine = s1_rows(step, 0, 1 - x) if by_side(step) else s1_rows(step, 1, x)
         s2[step] = (mine[...].astype(f32) + first_in[step, 0].astype(f32)).astype(bf16)
         wires.send(s2.at[step], mid_in.at[step], mid_at + step, across if by_side(step) else side)
 
     def sum_last(step):
-        wires.arrived(first_in.at[step, 1], first_at + 2 * step + 1, twin)
-        wires.arrived(mid_in.at[step], mid_at + step, twin)
+        wires.arrived(first_in.at[step, 1], first_at + 2 * step + 1)
+        wires.arrived(mid_in.at[step], mid_at + step)
         final[step] = (
             s1_rows(step, 0, x)[...].astype(f32) + first_in[step, 1].astype(f32) + mid_in[step].astype(f32)
         ).astype(bf16)
         if step == 0:
             part(back, z)[...] = final[0]
         else:
-            wires.send(final.at[step], part(back, z), home + step, {"ep": 2 * zfrom(step) + x, "tp": t})
-
-    loads[3].wait()
-    loads[4].wait()
-    from_twin(0)
-    from_twin(1)
-    expert_half(0)
-    for step in range(groups):
-        if step:
-            wires.arrived(wt_all.at[2 * step + x], z_wts + step, twin)
-        wires.arrived(wt_all.at[2 * step + 1 - x], wt_side + step, twin)
-    for i in range(2 * groups):
-        tiles = wt_all[i].astype(f32)
-        both = jnp.where(x == 0, tiles[0:1, :] + tiles[1:2, :], tiles[2:3, :] + tiles[3:4, :])
-        wt_col[i * cap:(i + 1) * cap, :] = jnp.transpose(jnp.broadcast_to(both, (128, 128)))[:cap, :]
-    loads[5].wait()
-    give_half(0)
-    from_second(2)
-    from_second(3)
-    wires.send(kv_s.at[z], kv_all.at[e], kv_side, across)
-    for step in range(1, groups):
-        kv_at = kv_all.at[2 * zfrom(step) + x]
-        wires.arrived(kv_at, z_kv + step, twin)
-        wires.send(kv_at, kv_at, kv_side + step, across)
-    sum_core(0)
-    from_twin(2)
-    from_twin(3)
-    expert_half(1)
-    give_half(1)
-    sum_core(1)
-    sum_first(0)
-    sum_first(1)
-
-    for step in range(groups):
-        wires.arrived(kv_all.at[2 * zfrom(step) + 1 - x], kv_side + step, twin)
-        for other in (0, 1):
-            if step or other:
-                xx = 1 - x if other else x
-                wires.arrived(q_all.at[2 * zfrom(step) + xx], q_in + 2 * step + other, twin)
+            wires.send(final.at[step], part(back, z), home, {"ep": 2 * zfrom(step) + x, "tp": t})
+
+    def take_weights():
+        wires.arrived(wt_all.at[pl.ds(0, 2 * groups - 1)], wt_in)
+        for i in range(2 * groups):
+            tiles = wt_all[i].astype(f32)
+            both = jnp.where(x == 0, tiles[0:1, :] + tiles[1:2, :], tiles[2:3, :] + tiles[3:4, :])
+            wt_col[i * cap:(i + 1) * cap, :] = jnp.transpose(jnp.broadcast_to(both, (128, 128)))[:cap, :]
+
     blocks = 2 * groups
-    acc[...] = jnp.zeros_like(acc)
-    kept[...] = jnp.zeros_like(kept)
-    offset = off_ref[z]
     later = jnp.where(row > lane, 1.0, 0.0).astype(bf16)
-    for kb in reversed(range(blocks)):
+    att_in = wires.take(groups)
+    att_side = wires.take(groups)
+    att_twin = wires.take(1)
+
+    def att_at(rows_at, tt, hh):
+        return att.at[rows_at, pl.ds(pl.multiple_of(tt * narrow + hh * HD, HD), HD)]
+
+    def take_kv():
+        wires.arrived(kv_all.at[pl.ds(0, groups)], kv_side)
+        wires.arrived(q_all.at[pl.ds(0, blocks - 1)], q_in)
+        loads["off"].wait()
+
+    def attend(kb):
         low = kb * cap
         size = blocks * cap - low
-        if kb == 1:
-            sum_first(2)
-            sum_first(3)
         queries = q_all[kb:, :, :].reshape(size, HD)
         scores = lax.dot_general(
             queries, kv_all[kb, :, :HD], (((1,), (1,)), ((), ())), preferred_element_type=f32
         )
-        scores = scores * HD ** (-0.5) + offset
+        scores = scores * HD ** (-0.5) + off_ref[z]
         r_at = lax.broadcasted_iota(jnp.int32, (size, rows), 0)
         s_at = lax.broadcasted_iota(jnp.int32, (size, rows), 1)
         causal = (r_at >= cap) | (s_at < r_at + x * cap)
@@ -559,55 +538,103 @@
         )
         wts = jnp.where(causal, jnp.exp(scores + keep + within), 0.0).astype(bf16)
         out = jnp.dot(wts, kv_all[kb, :, HD:], preferred_element_type=f32)
-        sofar = kept[low:, :]
-        acc[low:, :] = acc[low:, :] + jnp.exp(sofar) * out
-        kept[low:, :] = sofar + (within[:, 0:1] + masked[:, 0:1])
-    att_s[...] = acc[...].astype(bf16)
-
-    def att_at(hh, xx):
-        return att.at[half(xx), pl.ds(pl.multiple_of(t * narrow + hh * HD, HD), HD)]
-
-    att_in = wires.take(2 * groups)
-    for step in range(groups):
-        for other in (0, 1):
-            if step or other:
-                xx = 1 - x if other else x
-                wires.send(
-                    part(att_s, 2 * zto(step) + xx), att_at(z, x), att_in + 2 * step + other, peer(step, other)
-                )
-    att_at(z, x)[...] = part(att_s, e)[...]
-
+        if kb:
+            out = acc[low:, :] * jnp.exp(within[:, 0:1] + masked[:, 0:1]) + out
+        acc[low:, :] = out
+        att_s[low:low + cap, :] = out[:cap, :].astype(bf16)
+
+        @pl.when(e == kb)
+        def _():
+            att_at(half(x), t, z)[...] = att_s[low:low + cap, :]
+
+        @pl.when(e != kb)
+        def _():
+            wires.send(
+                att_s.at[low:low + cap, :], att_at(half(x), t, z), att_in + z, {"ep": kb, "tp": t}
+            )
+
+        if kb == 0:
+            wires.sent_bytes -= cap * HD * 2
+
+    def share_att(step):
+        piece = att_at(slice(None), t, zfrom(step))
+        like = piece if step else att_at(slice(0, cap), t, z)
+        wires.arrived(like, att_in + zfrom(step))
+        wires.send(piece, piece, att_side + step, side)
+        wires.send(piece, piece, att_twin, twin)
+
+    def pass_att(step):
+        piece = att_at(slice(None), ty, zfrom(step))
+        wires.arrived(piece, att_side + step)
+        wires.send(piece, piece, att_twin, twin)
+
+    from_first(0)
+    from_z(1)
+    from_second(0)
+    from_z(2)
+    from_first(1)
+    from_z(3)
+    from_third(0)
+    pass_kv(1)
+    from_second(1)
+    from_first(2)
+    pass_kv(2)
+    pass_kv(3)
+    from_third(1)
+    from_second(2)
+    from_first(3)
+    take_weights()
+    loads["gate"].wait()
+    loads["up"].wait()
+    loads["down"].wait()
+    from_twin(0)
+    from_twin(1)
+    expert_tile(0, 0)
+    from_third(2)
+    from_second(3)
+    expert_tile(0, 1)
+    from_third(3)
+    give_half(0)
+    sum_core(0)
+    take_kv()
+    for kb in range(4):
+        attend(kb)
+    from_twin(2)
+    from_twin(3)
+    expert_tile(1, 0)
+    expert_tile(1, 1)
+    sum_first(0)
+    sum_first(1)
+    give_half(1)
+    sum_core(1)
+    attend(4)
+    sum_last(0)
     sum_last(1)
-    sum_last(0)
-
-    for step in range(groups):
-        for other in (0, 1):
-            if step or other:
-                xx = 1 - x if other else x
-                wires.arrived(att_at(zfrom(step), xx), att_in + 2 * step + other, twin)
-
-    def att_cols(tt):
-        return att.at[:, pl.ds(pl.multiple_of(tt * narrow, 128), narrow)]
-
-    att_go = wires.take(3)
-    wires.send(att_cols(t), att_cols(t), att_go, side)
-    wires.send(att_cols(t), att_cols(t), att_go + 1, twin)
-
+    attend(5)
+    attend(6)
+    sum_first(2)
+    sum_first(3)
+    attend(7)
+    share_att(0)
+    share_att(1)
+    share_att(3)
+    share_att(2)
     sum_last(2)
     sum_last(3)
-    wires.arrived(att_cols(ty), att_go, twin)
-    wires.send(att_cols(ty), att_cols(ty), att_go + 2, twin)
-    loads[6].wait()
-    wires.arrived(att_cols(tc), att_go + 1, twin)
-    wires.arrived(att_cols(tyc), att_go + 2, twin)
+    pass_att(0)
+    pass_att(1)
+    pass_att(3)
+    pass_att(2)
+    loads["wo"].wait()
+    wires.arrived(att.at[:, pl.ds(0, 2 * narrow)], att_twin)
     for cut in range(2):
         at = slice(cut * tile, (cut + 1) * tile)
         mix_ref[:, at] = jnp.dot(att[...], wo[:, at], preferred_element_type=f32).astype(bf16)
-
-    for step in range(1, groups):
-        wires.arrived(part(back, zto(step)), home + step, twin)
+    wires.arrived(back.at[pl.ds(0, (groups - 1) * cap), :], home)
     exp_ref[...] = jnp.dot(pick[...], back[...], preferred_element_type=f32).astype(bf16)
-    wires.drain()
+    wires.drain(weights)
+    wt_sent = wt_all.at[pl.ds(0, 2 * groups - 1)]
+    pltpu.make_async_copy(wt_sent, wt_sent, send_sem.at[1]).wait()
 
 
 def fused_on_device(
@@ -622,16 +649,18 @@
     pool = groups * cap
     heads = narrow // HD
     ff = gate_weight.shape[2]
-    vmem = pl.BlockSpec(memory_space=pltpu.VMEM)
-    smem = pl.BlockSpec(memory_space=pltpu.SMEM)
-    hbm = pl.BlockSpec(memory_space=pl.ANY)
+    hbm = pl.BlockSpec(memory_space=pltpu.HBM)
     scratch = [
-        pltpu.VMEM((3, width, narrow), bf16),
-        pltpu.VMEM((width, narrow), bf16),
-        pltpu.VMEM((width, ff), bf16),
-        pltpu.VMEM((width, ff), bf16),
+        pltpu.VMEM((rows, width), bf16),
+        pltpu.VMEM((1, width), f32),
+        pltpu.SMEM((heads,), f32),
+        pltpu.VMEM((rows, width), bf16),
+        pltpu.VMEM((1, width), f32),
+        pltpu.VMEM((2, rows), jnp.int32),
+        pltpu.VMEM((2, rows), f32),
+        pltpu.VMEM((6 * width, narrow), bf16),
         pltpu.VMEM((ff, width), bf16),
-        pltpu.SemaphoreType.DMA((7,)),
+        pltpu.SemaphoreType.DMA((LOADS,)),
         pltpu.VMEM((rows, width), bf16),
         pltpu.VMEM((rows, pool), bf16),
         pltpu.VMEM((pool, narrow), bf16),
@@ -643,7 +672,6 @@
         pltpu.VMEM((heads, rows, HD), bf16),
         pltpu.VMEM((2 * groups, rows, 2 * HD), bf16),
         pltpu.VMEM((2 * groups, cap, HD), bf16),
-        pltpu.VMEM((2 * pool, HD), f32),
         pltpu.VMEM((2 * pool, HD), f32),
         pltpu.VMEM((2 * pool, HD), bf16),
         pltpu.VMEM((rows, width), bf16),
@@ -657,24 +685,24 @@
         pltpu.VMEM((groups, cap, narrow), bf16),
         pltpu.VMEM((groups, cap, narrow), bf16),
         pltpu.VMEM((pool, narrow), bf16),
-        pltpu.SemaphoreType.DMA((WIRES,)),
+        pltpu.SemaphoreType.DMA((2,)),
         pltpu.SemaphoreType.DMA((WIRES,)),
     ]
     both = pl.pallas_call(
         functools.partial(fused_kernel, groups),
-        out_shape=jax.ShapeDtypeStruct((2, rows, narrow), bf16),
-        in_specs=[vmem, vmem, hbm, hbm, hbm, smem, hbm, vmem, vmem, vmem, vmem, hbm, hbm, hbm],
-        out_specs=vmem,
+        out_shape=pltpu.VMEM((2, rows, narrow), bf16),
+        in_specs=[hbm] * 14,
+        out_specs=pl.BlockSpec(memory_space=pltpu.VMEM),
         scratch_shapes=scratch,
         compiler_params=pltpu.CompilerParams(
-            collective_id=0, has_side_effects=True, vmem_limit_bytes=56 * 1024 * 1024
+            collective_id=0, has_side_effects=True, vmem_limit_bytes=48 * 1024 * 1024
         ),
         name="fused",
-    )(
+    )(*(pltpu.with_memory_space_constraint(value, pltpu.HBM) for value in (
         mixer_input, mixer_gain.reshape(1, width), query_weight, key_weight, value_weight, score_offset,
         out_weight, expert_input, expert_gain.reshape(1, width), route_ids.T, route_weights.T,
         gate_weight, up_weight, down_weight,
-    )
+    )))
     return both[0], both[1]
 
 

time: 52.4 us -> 47.7 us (0.910)
  Pallas kernels: 49.9 us -> 46.2 us
  local copies, waits for them, and re-layouts: 1.68 us -> 0.72 us
    pallas_call x1, Pallas kernels: 49.9 us -> 46.2 us  [fused_on_device(): pl.pallas_call(functools.partial(fused_kernel, groups), out_shape=pltpu.V...]
    squeeze x1, local copies, waits for them, and re-layouts: 1.68 us -> 0.72 us  [fused_on_device(): return (both[0], both[1])]
where the time goes in v1:
time: 47.7 us; the launch traced here: 47.6 us
  Pallas kernels  46.2 us (97%)
  local copies, waits for them, and re-layouts  0.72 us (2%)
  between operations  0.64 us (1%)
    pallas_call x1, Pallas kernels, fused_on_device(): pl.pallas_call(functools.partial(fused_kernel, groups), out_shape=pltpu.V...  46.2 us

profile of v1, /device:TPU:0, one launch (start us, length us, event | category | flops | bytes accessed | tf_op | source)
XLA Modules:
  0.0 47.6 jit_solution(18136345704523101441)
XLA Ops:
  0.6 46.2 %fused.1 = bf16[2,128,512]{2,1,0:T(8,128)(2,1)S(1)} custom-call(bf16[128,2048]{1,0:T(8,128)(2,1)} %xa_hbm.1, f32[1,2048]{1,0:T(1,128)} %bitcast.8, bf16[2048,512]{1,0:T(8,128)(2,1)} %wq_hbm.1, bf16[2048,512]{1,0:T(8,128)(2,1)} %wk_hbm.1, bf16[2048,512]{1,0:T(8,128)(2,1)} %wv_hbm.1, f32[4]{0:T(128)} %off_hbm.1, bf16[2048,512]{1,0:T(8,128)(2,1)} %wo_hbm.1, ...), custom_call_target="tpu_custom_call" | custom-call | tf_op jit(solution)/shard_map/fused/pallas_call | solution.py:691
  46.9 0.7 %slice_bitcast_fusion = (bf16[128,512]{1,0:T(8,128)(2,1)}, bf16[128,512]{1,0:T(8,128)(2,1)}) fusion(bf16[2,128,512]{2,1,0:T(8,128)(2,1)S(1)} %fused.1), kind=kLoop, calls=%fused_computation | loop fusion | bytes 524288 | tf_op jit(solution)/shard_map/squeeze | solution.py:706
